TPU v7x, 256 devices: a whole 4x4x8 slice. The times are simulated.
256 devices in a mesh: ra: 16 (over y, x), cb: 16 (over z, core).
Axes of the slice: x: 4, y: 4, z: 8, core: 2. Of those that a mesh axis runs over, the one named last changes fastest.
Arguments:
- hidden_states: bfloat16 [384, 4096], P(None, 'ra'), may hold values from -40 to 40
- gain_first: bfloat16 [4096], P('ra'), may hold values from 0.099609375 to 1.8984375
- gate_first: bfloat16 [4096, 11264], P('ra', 'cb'), may hold values from -0.09375 to 0.09375
- up_first: bfloat16 [4096, 11264], P('ra', 'cb'), may hold values from -0.09375 to 0.09375
- down_first: bfloat16 [11264, 4096], P('cb', 'ra'), may hold values from -0.0546875 to 0.0546875
- gain_second: bfloat16 [4096], P('ra'), may hold values from 0.099609375 to 1.8984375
- gate_second: bfloat16 [4096, 11264], P('ra', 'cb'), may hold values from -0.09375 to 0.09375
- up_second: bfloat16 [4096, 11264], P('ra', 'cb'), may hold values from -0.09375 to 0.09375
- down_second: bfloat16 [11264, 4096], P('cb', 'ra'), may hold values from -0.0546875 to 0.0546875
- gain_last: bfloat16 [4096], P('ra'), may hold values from 0.099609375 to 1.8984375
Outputs:
- closed: bfloat16 [384, 4096], P(None, 'ra')
All inputs are finite; a program needn't handle non-finite values.
Results may differ from a plain program's by a relative error of at most 0.0098.
Values may be sent and summed in bfloat16 or wider, within the bound.
A program may use at most 64 MiB of HBM per device.

v0:
```python
import jax
import jax.numpy as jnp
from jax import lax
from jax.sharding import Mesh
from jax.sharding import PartitionSpec as P

D = 4096
RA = ("ra_0", "ra_1")


norm_eps = 1e-06
residual_weight = 0.25
branch_weight = 0.5


def in_blocks(value, dim, length):
    before, after = (value.shape[:dim], value.shape[dim + 1 :])
    return jnp.moveaxis(value.reshape(*before, length, -1, *after), dim, 0)


def sum_at_owner(value, axis, dim):
    length = lax.axis_size(axis)
    blocks = lax.all_to_all(in_blocks(value, dim, length), axis, 0, 0, tiled=True)
    return jnp.sum(blocks, axis=0)


def sent_together(arrays, axis, dim, along):
    widths = [a.shape[along] for a in arrays]
    both = jnp.concatenate(arrays, axis=along)
    filled = sum_at_owner(both, axis, dim)
    return tuple(jnp.split(filled, [sum(widths[:k]) for k in range(1, len(widths))], axis=along))


def from_everyone(value, axis):
    length = lax.axis_size(axis)
    return lax.all_to_all(
        jnp.broadcast_to(value[None], (length, *value.shape)), axis, 0, 0, tiled=True
    )


def laid_out(blocks, dim):
    shape = list(blocks.shape[1:])
    shape[dim] *= blocks.shape[0]
    return jnp.moveaxis(blocks, 0, dim).reshape(shape)


def gather_directly(value, axis, dim):
    blocks = from_everyone(value, axis)
    return laid_out(blocks, dim)


def over_axes(value, axes):
    for axis in axes:
        value = lax.psum(value, axis)
    return value


def half_step(stream, gain, w_gate, w_up, w_down):
    values = stream.astype(jnp.float32)
    local_squares = jnp.sum(values * values, axis=1)
    normed = (values * gain.astype(jnp.float32)).astype(jnp.bfloat16)
    gate_part = jnp.dot(normed, w_gate, preferred_element_type=jnp.float32)
    upper_part = jnp.dot(normed, w_up, preferred_element_type=jnp.float32)
    gate, upper, squares = sent_together((gate_part, upper_part, local_squares[:, None]), RA, 0, 1)
    scale = lax.rsqrt(squares / D + norm_eps)
    hidden = (jax.nn.silu(gate * scale) * (upper * scale)).astype(jnp.bfloat16)
    branch = jnp.dot(gather_directly(hidden, RA, 0), w_down, preferred_element_type=jnp.float32)
    block = sum_at_owner(branch, "cb", 0)
    count = block.shape[0]
    offset = lax.axis_index("cb") * count
    own_rows = lax.dynamic_slice_in_dim(values, offset, count, 0)
    updated = (residual_weight * own_rows + branch_weight * block).astype(jnp.bfloat16)
    return gather_directly(updated, "cb", 0)


def body(
    hidden_states,
    gain_first,
    gate_first,
    up_first,
    down_first,
    gain_second,
    gate_second,
    up_second,
    down_second,
    gain_last,
):
    first = half_step(hidden_states, gain_first, gate_first, up_first, down_first)
    second = half_step(first, gain_second, gate_second, up_second, down_second)
    values = second.astype(jnp.float32)
    squares = over_axes(jnp.sum(values * values, axis=1), RA)
    scale = lax.rsqrt(squares / D + norm_eps)[:, None]
    return (values * scale * gain_last.astype(jnp.float32)).astype(jnp.bfloat16)


def solution(mesh):
    split = Mesh(mesh.devices.reshape(4, 4, mesh.shape["cb"]), ("ra_0", "ra_1", "cb"))
    return jax.shard_map(
        body,
        mesh=split,
        in_specs=(
            P(None, RA),
            P(RA),
            P(RA, "cb"),
            P(RA, "cb"),
            P("cb", RA),
            P(RA),
            P(RA, "cb"),
            P(RA, "cb"),
            P("cb", RA),
            P(RA),
        ),
        out_specs=P(None, RA),
        check_vma=False,
    )
```

profile of v0, /device:TPU:1, one launch (start us, length us, event | category | flops | bytes accessed | tf_op | source)
XLA Modules:
  0.0 209.0 jit_solution(11229459971690430254)
XLA Ops:
  0.0 0.7 convert_element_type.56
  0.7 1.1 multiply_reduce_fusion.2
  1.8 2.3 %fusion.11 = f32[384,704]{1,0:T(8,128)} fusion(bf16[256,704]{0,1:T(8,128)(2,1)S(1)} %copy-done, f32[256]{0:T(256)S(1)} %convert_element_type.56, bf16[384,256]{1,0:T(8,128)(2,1)} %param.10), kind=kOutput, calls=%fused_computation.17 | convolution fusion | flops 138706944 | bytes 1639424 | tf_op jit(solution)/shard_map/dot_general | solution.py:62
  4.1 1.4 fusion.10
  5.5 0.2 concatenate.22
  5.7 2.7 %concatenate.19 = f32[16,24,1409]{2,1,0:T(8,128)S(1)} concatenate(f32[16,24,704]{2,1,0:T(8,128)} %bitcast.28, f32[16,24,704]{2,1,0:T(8,128)} %bitcast.29, f32[16,24,1]{2,1,0:T(8,128)S(1)} %concatenate.22), dimensions={2} | concatenate | bytes 4328448 | tf_op jit(solution)/shard_map/concatenate | solution.py:29
  8.5 37.9 %all_to_all.40 = f32[16,24,1409]{2,1,0:T(8,128)} all-to-all(f32[16,24,1409]{2,1,0:T(8,128)S(1)} %concatenate.19), channel_id=1, replica_groups=mesh['ra_0'=4,'ra_1'=4,'cb'=16] {'ra_0','ra_1'}, dimensions={0} | all-to-all | bytes 4328448 | tf_op jit(solution)/shard_map/all_to_all | solution.py:23
  46.3 1.8 reduce_sum.66
  48.4 14.2 %all_to_all.41 = bf16[16,24,704]{2,1,0:T(8,128)(2,1)S(1)} all-to-all(bf16[16,24,704]{2,1,0:T(8,128)(2,1)S(1)} %broadcast_in_dim.8), channel_id=1, replica_groups=mesh['ra_0'=4,'ra_1'=4,'cb'=16] {'ra_0','ra_1'}, dimensions={0} | all-to-all | bytes 1081344 | tf_op jit(solution)/shard_map/all_to_all | solution.py:36
  62.7 1.1 fusion.8
  63.7 10.7 %all-to-all-start.2 = ((f32[16,24,256]{2,1,0:T(8,128)}), f32[16,24,256]{2,1,0:T(8,128)S(1)}, u32[]{:S(2)}, u32[]{:S(2)}) async-start(f32[16,24,256]{2,1,0:T(8,128)} %fusion.8), calls=%async_computation.2 | async-start | bytes 786432 | tf_op jit(solution)/shard_map/all_to_all | solution.py:23
  74.5 14.4 %all-to-all-done.2 = f32[16,24,256]{2,1,0:T(8,128)S(1)} async-done(((f32[16,24,256]{2,1,0:T(8,128)}), f32[16,24,256]{2,1,0:T(8,128)S(1)}, u32[]{:S(2)}, u32[]{:S(2)}) %all-to-all-start.2) | async-done | bytes 393248 | tf_op jit(solution)/shard_map/all_to_all | solution.py:23
  89.0 0.7 broadcast_in_dim.9
  89.7 3.6 %all-to-all-start.3 = ((bf16[16,24,256]{2,1,0:T(8,128)(2,1)}), bf16[16,24,256]{2,1,0:T(8,128)(2,1)S(1)}, u32[]{:S(2)}, u32[]{:S(2)}) async-start(bf16[16,24,256]{2,1,0:T(8,128)(2,1)} %broadcast_in_dim.9), calls=%async_computation.3 | async-start | bytes 393216 | tf_op jit(solution)/shard_map/all_to_all | solution.py:36
  93.3 9.6 %all-to-all-done.3 = bf16[16,24,256]{2,1,0:T(8,128)(2,1)S(1)} async-done(((bf16[16,24,256]{2,1,0:T(8,128)(2,1)}), bf16[16,24,256]{2,1,0:T(8,128)(2,1)S(1)}, u32[]{:S(2)}, u32[]{:S(2)}) %all-to-all-start.3) | async-done | bytes 196640 | tf_op jit(solution)/shard_map/all_to_all | solution.py:36
  102.9 0.1 multiply_reduce_fusion.1
  103.0 0.2 copy.31
  103.2 1.4 fusion.4
  104.6 1.4 fusion.6
  106.0 2.7 %concatenate.21 = f32[16,24,1409]{2,1,0:T(8,128)S(1)} concatenate(f32[16,24,704]{2,1,0:T(8,128)} %fusion.6, f32[16,24,704]{2,1,0:T(8,128)} %fusion.4, f32[16,24,1]{2,1,0:T(8,128)S(1)} %copy.31), dimensions={2} | concatenate | bytes 4328448 | tf_op jit(solution)/shard_map/concatenate | solution.py:29
  108.7 34.5 %all_to_all.42 = f32[16,24,1409]{2,1,0:T(8,128)} all-to-all(f32[16,24,1409]{2,1,0:T(8,128)S(1)} %concatenate.21), channel_id=1, replica_groups=mesh['ra_0'=4,'ra_1'=4,'cb'=16] {'ra_0','ra_1'}, dimensions={0} | all-to-all | bytes 4328448 | tf_op jit(solution)/shard_map/all_to_all | solution.py:23
  143.2 1.8 reduce_sum.69
  145.3 14.0 %all_to_all.43 = bf16[16,24,704]{2,1,0:T(8,128)(2,1)S(1)} all-to-all(bf16[16,24,704]{2,1,0:T(8,128)(2,1)S(1)} %broadcast_in_dim.10), channel_id=1, replica_groups=mesh['ra_0'=4,'ra_1'=4,'cb'=16] {'ra_0','ra_1'}, dimensions={0} | all-to-all | bytes 1081344 | tf_op jit(solution)/shard_map/all_to_all | solution.py:36
  159.3 1.1 fusion.2
  160.3 5.5 %all-to-all-start.6 = ((f32[16,24,256]{2,1,0:T(8,128)}), f32[16,24,256]{2,1,0:T(8,128)S(1)}, u32[]{:S(2)}, u32[]{:S(2)}) async-start(f32[16,24,256]{2,1,0:T(8,128)} %fusion.2), calls=%async_computation.6 | async-start | bytes 786432 | tf_op jit(solution)/shard_map/all_to_all | solution.py:23
  165.9 14.5 %all-to-all-done.6 = f32[16,24,256]{2,1,0:T(8,128)S(1)} async-done(((f32[16,24,256]{2,1,0:T(8,128)}), f32[16,24,256]{2,1,0:T(8,128)S(1)}, u32[]{:S(2)}, u32[]{:S(2)}) %all-to-all-start.6) | async-done | bytes 393248 | tf_op jit(solution)/shard_map/all_to_all | solution.py:23
  180.4 0.7 broadcast_in_dim.11
  181.1 3.4 %all-to-all-start.7 = ((bf16[16,24,256]{2,1,0:T(8,128)(2,1)}), bf16[16,24,256]{2,1,0:T(8,128)(2,1)S(1)}, u32[]{:S(2)}, u32[]{:S(2)}) async-start(bf16[16,24,256]{2,1,0:T(8,128)(2,1)} %broadcast_in_dim.11), calls=%async_computation.7 | async-start | bytes 393216 | tf_op jit(solution)/shard_map/all_to_all | solution.py:36
  184.6 9.6 %all-to-all-done.7 = bf16[16,24,256]{2,1,0:T(8,128)(2,1)S(1)} async-done(((bf16[16,24,256]{2,1,0:T(8,128)(2,1)}), bf16[16,24,256]{2,1,0:T(8,128)(2,1)S(1)}, u32[]{:S(2)}, u32[]{:S(2)}) %all-to-all-start.7) | async-done | bytes 196640 | tf_op jit(solution)/shard_map/all_to_all | solution.py:36
  194.4 6.8 %psum.14 = f32[384]{0:T(512)S(1)} all-reduce(f32[384]{0:T(512)S(1)} %reduce_sum.72), channel_id=1, replica_groups=mesh['ra_0'=4,'ra_1'=4,'cb'=16] {'ra_0'}, use_global_device_ids=true, to_apply=%region_7.8 | all-reduce | flops 384 | bytes 3072 | tf_op jit(solution)/shard_map/psum | solution.py:54
  201.2 6.9 %psum.15 = f32[384]{0:T(512)S(1)} all-reduce(f32[384]{0:T(512)S(1)} %psum.14), channel_id=1, replica_groups=mesh['ra_0'=4,'ra_1'=4,'cb'=16] {'ra_1'}, use_global_device_ids=true, to_apply=%region_8.9 | all-reduce | flops 384 | bytes 3072 | tf_op jit(solution)/shard_map/psum | solution.py:54
  208.2 0.8 fusion.1
  (35 shorter events, 0.9 us)
Async XLA Ops:
  0.0 1.8 copy-start
  0.0 4.1 %copy-start.1 = (bf16[384,256]{1,0:T(8,128)(2,1)S(1)}, bf16[384,256]{1,0:T(8,128)(2,1)}, u32[]{:S(2)}) copy-start(bf16[384,256]{1,0:T(8,128)(2,1)} %param.10) | copy-start | bytes 589828
  0.0 4.1 %copy-start.2 = (bf16[256,704]{0,1:T(8,128)(2,1)S(1)}, bf16[256,704]{0,1:T(8,128)(2,1)}, u32[]{:S(2)}) copy-start(bf16[256,704]{0,1:T(8,128)(2,1)} %param.13) | copy-start | bytes 1081348
  48.1 14.5 %copy-start.3 = (bf16[704,256]{1,0:T(8,128)(2,1)S(1)}, bf16[704,256]{1,0:T(8,128)(2,1)}, u32[]{:S(2)}) copy-start(bf16[704,256]{1,0:T(8,128)(2,1)} %param.14) | copy-start | bytes 1081348
  63.7 29.5 %copy-start.7 = (bf16[256]{0:T(256)(128)(2,1)S(1)}, bf16[256]{0:T(256)(128)(2,1)}, u32[]{:S(2)}) copy-start(bf16[256]{0:T(256)(128)(2,1)} %param.15) | copy-start | bytes 1540
  63.7 25.2 %all-to-all-start.2 = ((f32[16,24,256]{2,1,0:T(8,128)}), f32[16,24,256]{2,1,0:T(8,128)S(1)}, u32[]{:S(2)}, u32[]{:S(2)}) async-start(f32[16,24,256]{2,1,0:T(8,128)} %fusion.8), calls=%async_computation.2 | async-start | bytes 786432 | tf_op jit(solution)/shard_map/all_to_all | solution.py:23
  74.5 28.7 %copy-start.4 = (bf16[256,704]{0,1:T(8,128)(2,1)S(1)}, bf16[256,704]{0,1:T(8,128)(2,1)}, u32[]{:S(2)}) copy-start(bf16[256,704]{0,1:T(8,128)(2,1)} %param.17) | copy-start | bytes 1081348
  89.7 14.9 %copy-start.5 = (bf16[256,704]{0,1:T(8,128)(2,1)S(1)}, bf16[256,704]{0,1:T(8,128)(2,1)}, u32[]{:S(2)}) copy-start(bf16[256,704]{0,1:T(8,128)(2,1)} %param.16) | copy-start | bytes 1081348
  89.7 13.2 %all-to-all-start.3 = ((bf16[16,24,256]{2,1,0:T(8,128)(2,1)}), bf16[16,24,256]{2,1,0:T(8,128)(2,1)S(1)}, u32[]{:S(2)}, u32[]{:S(2)}) async-start(bf16[16,24,256]{2,1,0:T(8,128)(2,1)} %broadcast_in_dim.9), calls=%async_computation.3 | async-start | bytes 393216 | tf_op jit(solution)/shard_map/all_to_all | solution.py:36
  145.0 14.3 %copy-start.6 = (bf16[704,256]{1,0:T(8,128)(2,1)S(1)}, bf16[704,256]{1,0:T(8,128)(2,1)}, u32[]{:S(2)}) copy-start(bf16[704,256]{1,0:T(8,128)(2,1)} %param.18) | copy-start | bytes 1081348
  160.3 24.2 %copy-start.8 = (bf16[256]{0:T(256)(128)(2,1)S(1)}, bf16[256]{0:T(256)(128)(2,1)}, u32[]{:S(2)}) copy-start(bf16[256]{0:T(256)(128)(2,1)} %param.19) | copy-start | bytes 1540
  160.3 20.1 %all-to-all-start.6 = ((f32[16,24,256]{2,1,0:T(8,128)}), f32[16,24,256]{2,1,0:T(8,128)S(1)}, u32[]{:S(2)}, u32[]{:S(2)}) async-start(f32[16,24,256]{2,1,0:T(8,128)} %fusion.2), calls=%async_computation.6 | async-start | bytes 786432 | tf_op jit(solution)/shard_map/all_to_all | solution.py:23
  181.1 13.0 %all-to-all-start.7 = ((bf16[16,24,256]{2,1,0:T(8,128)(2,1)}), bf16[16,24,256]{2,1,0:T(8,128)(2,1)S(1)}, u32[]{:S(2)}, u32[]{:S(2)}) async-start(bf16[16,24,256]{2,1,0:T(8,128)(2,1)} %broadcast_in_dim.11), calls=%async_computation.7 | async-start | bytes 393216 | tf_op jit(solution)/shard_map/all_to_all | solution.py:36
where the time goes:
time: 212 us; the launch traced here: 209 us
  blocking collectives  114 us (54%)
  waiting for transfers between devices  48.1 us (23%)
  starting transfers between devices  23.3 us (11%)
  matrix products  8.6 us (4%)
  local copies, waits for them, and re-layouts  7.42 us (4%)
  other arithmetic  7.07 us (3%)
    all_to_all x2, blocking collectives, sum_at_owner(): lax.all_to_all(in_blocks(value, dim, length), axis, 0, 0, tiled=True)  72.3 us
    all_to_all x2, waiting for transfers between devices, sum_at_owner(): lax.all_to_all(in_blocks(value, dim, length), axis, 0, 0, tiled=True)  28.9 us
    all_to_all x2, blocking collectives, from_everyone(): lax.all_to_all(jnp.broadcast_to(value[None], (length, *value.shape)), axi...  28.2 us
    all_to_all x2, waiting for transfers between devices, from_everyone(): lax.all_to_all(jnp.broadcast_to(value[None], (length, *value.shape)), axi...  19.2 us
    all_to_all x2, starting transfers between devices, sum_at_owner(): lax.all_to_all(in_blocks(value, dim, length), axis, 0, 0, tiled=True)  16.3 us
    psum x2, blocking collectives, over_axes(): value = lax.psum(value, axis)  13.7 us
    all_to_all x2, starting transfers between devices, from_everyone(): lax.all_to_all(jnp.broadcast_to(value[None], (length, *value.shape)), axi...  6.97 us
    concatenate x4, local copies, waits for them, and re-layouts, sent_together(): both = jnp.concatenate(arrays, axis=along)  5.83 us
  transfers between devices with their start and end apart: 4, of which 4 were waited for; matrix products, arithmetic and copies ran while one was open for 0% of the time, Pallas kernels for 0%

commit v1 on v0

v1 whole, which is shorter than its diff:
```python
import functools

import jax
import jax.numpy as jnp
from jax import lax
from jax.experimental import pallas as pl
from jax.experimental.pallas import tpu as pltpu
from jax.sharding import PartitionSpec as P

MESH = pl.DeviceIdType.MESH
F32, BF16 = jnp.float32, jnp.bfloat16

D = 4096
NORM_EPS = 1e-06
RESIDUAL_WEIGHT = 0.25
BRANCH_WEIGHT = 0.5

N = 16
CHUNKS = 3
PAD = 64


def kernel(
    x_hbm, g1, g2, g3, wg1, wu1, wd1, wg2, wu2, wd2, out,
    x, gain1, gain2, gain3, wg, wu, wd, part, part_in, hid, down, down_in, own, first, sq, sq_in,
    load_sem, send_sem, recv_sem,
):
    ra, cb = lax.axis_index("ra"), lax.axis_index("cb")
    rows, width = x.shape[1:]
    units = wg.shape[1]
    half = units + PAD
    tokens = N * rows

    loads = [
        pltpu.make_async_copy(src, dst, load_sem.at[i])
        for i, (src, dst) in enumerate([
            (x_hbm, x), (g1, gain1), (wg1, wg.at[0]), (wu1, wu.at[0]), (wd1, wd.at[0]),
            (g2, gain2), (wg2, wg.at[1]), (wu2, wu.at[1]), (wd2, wd.at[1]), (g3, gain3),
        ])
    ]
    for load in loads:
        load.start()

    def ra_peer(k):
        return {"ra": lax.rem(ra + k, N)}

    def cb_peer(k):
        return {"cb": lax.rem(cb + k, N)}

    barrier = pltpu.get_barrier_semaphore()
    for k in range(1, N):
        pl.semaphore_signal(barrier, inc=1, device_id=ra_peer(k), device_id_type=MESH)
        pl.semaphore_signal(barrier, inc=1, device_id=cb_peer(k), device_id_type=MESH)

    sent = []

    def send(peer, source, target, block, slot):
        index = len(sent)
        for k in range(1, N):
            pltpu.make_async_remote_copy(
                src_ref=source(k), dst_ref=target(k),
                send_sem=send_sem.at[index], recv_sem=recv_sem.at[index],
                device_id=peer(k), device_id_type=MESH,
            ).start()
        every = pltpu.make_async_remote_copy(
            src_ref=block, dst_ref=block,
            send_sem=send_sem.at[index], recv_sem=recv_sem.at[index],
            device_id=peer(1), device_id_type=MESH,
        )
        sent.append(every)
        return every.wait_recv

    def project(b, c, values, gain):
        squares = jnp.sum(values * values, axis=2, keepdims=True)
        normed = (values * gain[...].astype(F32).reshape(1, 1, width)).reshape(tokens, width).astype(BF16)
        for at, w in ((0, wg), (half, wu)):
            product = lax.dot_general(normed, w[b], (((1,), (1,)), ((), ())), preferred_element_type=F32)
            part[b, c, :, :, at : at + units] = product.reshape(N, rows, units).astype(BF16)
        high = squares.astype(BF16)
        low = (squares - high.astype(F32)).astype(BF16)
        part[b, c, :, :, units:half] = jnp.broadcast_to(high, (N, rows, PAD))
        part[b, c, :, :, half + units :] = jnp.broadcast_to(low, (N, rows, PAD))

    def send_parts(b, c):
        return send(
            ra_peer, lambda k: part.at[b, c, lax.rem(ra + k, N)], lambda k: part_in.at[b, c, k - 1],
            part_in.at[b, c], None,
        )

    def gate(b, c):
        total = part[b, c, ra].astype(F32)
        for k in range(N - 1):
            total += part_in[b, c, k].astype(F32)
        squares = total[:, units : units + 1] + total[:, half + units : half + units + 1]
        scale = lax.rsqrt(squares / D + NORM_EPS)
        g, u = total[:, :units] * scale, total[:, half : half + units] * scale
        hid[b, c, ra] = (g / (1.0 + jnp.exp(-g)) * u).astype(BF16)
        return send(
            ra_peer, lambda k: hid.at[b, c, ra], lambda k: hid.at[b, c, ra],
            hid.at[b, c, pl.ds(0, N - 1)], None,
        )

    def branch(b, c):
        rows_of_all = hid[b, c].astype(F32).reshape(tokens, units).astype(BF16)
        product = jnp.dot(rows_of_all, wd[b], preferred_element_type=F32)
        down[b, c] = product.reshape(N, rows, width).astype(BF16)
        return send(
            cb_peer, lambda k: down.at[b, c, lax.rem(cb + k, N)], lambda k: down_in.at[b, c, k - 1],
            down_in.at[b, c], None,
        )

    def updated(b, c, values):
        total = down[b, c, cb].astype(F32)
        for k in range(N - 1):
            total += down_in[b, c, k].astype(F32)
        return (RESIDUAL_WEIGHT * values.astype(F32) + BRANCH_WEIGHT * total).astype(BF16)

    chunks = range(CHUNKS)
    for load in loads[:4]:
        load.wait()
    waits = [None] * CHUNKS
    for c in chunks:
        project(0, c, x[pl.ds(c * N, N)].astype(F32), gain1)
        if c == 0:
            pl.semaphore_wait(barrier, 2 * (N - 1))
        waits[c] = send_parts(0, c)
    for c in chunks:
        waits[c]()
        waits[c] = gate(0, c)
    loads[4].wait()
    for c in chunks:
        waits[c]()
        waits[c] = branch(0, c)
    for c in chunks:
        waits[c]()
        first[c, cb] = updated(0, c, x[c * N + cb])
        waits[c] = send(
            cb_peer, lambda k: first.at[c, cb], lambda k: first.at[c, cb], first.at[c, pl.ds(0, N - 1)], None
        )
    for load in loads[5:8]:
        load.wait()
    for c in chunks:
        waits[c]()
        project(1, c, first[c].astype(F32), gain2)
        waits[c] = send_parts(1, c)
    for c in chunks:
        waits[c]()
        waits[c] = gate(1, c)
    for load in loads[8:]:
        load.wait()
    for c in chunks:
        waits[c]()
        waits[c] = branch(1, c)
    for c in chunks:
        waits[c]()
        second = updated(1, c, first[c, cb])
        own[c] = second
        values = second.astype(F32)
        sq[c] = jnp.broadcast_to(jnp.sum(values * values, axis=1, keepdims=True), sq.shape[1:])
        waits[c] = send(ra_peer, lambda k: sq.at[c], lambda k: sq_in.at[c, k - 1], sq_in.at[c], None)
    for c in chunks:
        waits[c]()
        squares = sq[c]
        for k in range(N - 1):
            squares += sq_in[c, k]
        scale = lax.rsqrt(squares[:, :1] / D + NORM_EPS)
        out[c * N + cb] = (own[c].astype(F32) * scale * gain3[...].astype(F32).reshape(1, width)).astype(BF16)
        waits[c] = send(
            cb_peer, lambda k: out.at[c * N + cb], lambda k: out.at[c * N + cb], out.at[pl.ds(0, N - 1)], None
        )
    for c in chunks:
        waits[c]()
    for every in sent:
        every.wait_send()


def body(
    hidden_states,
    gain_first,
    gate_first,
    up_first,
    down_first,
    gain_second,
    gate_second,
    up_second,
    down_second,
    gain_last,
):
    tokens, width = hidden_states.shape
    units = gate_first.shape[1]
    rows = tokens // (CHUNKS * N)
    x = hidden_states.reshape(CHUNKS * N, rows, width)
    gains = (gain_first, gain_second, gain_last)
    anywhere, vmem = pl.BlockSpec(memory_space=pltpu.HBM), pl.BlockSpec(memory_space=pltpu.VMEM)
    columns = 2 * (units + PAD)
    out = pl.pallas_call(
        kernel,
        out_shape=jax.ShapeDtypeStruct(x.shape, BF16),
        in_specs=[anywhere] * 10,
        out_specs=vmem,
        scratch_shapes=[
            pltpu.VMEM(x.shape, BF16),
            *[pltpu.VMEM((width,), BF16)] * 3,
            pltpu.VMEM((2, units, width), BF16),
            pltpu.VMEM((2, units, width), BF16),
            pltpu.VMEM((2, units, width), BF16),
            pltpu.VMEM((2, CHUNKS, N, rows, columns), BF16),
            pltpu.VMEM((2, CHUNKS, N - 1, rows, columns), BF16),
            pltpu.VMEM((2, CHUNKS, N, rows, units), BF16),
            pltpu.VMEM((2, CHUNKS, N, rows, width), BF16),
            pltpu.VMEM((2, CHUNKS, N - 1, rows, width), BF16),
            pltpu.VMEM((CHUNKS, rows, width), BF16),
            pltpu.VMEM((CHUNKS, N, rows, width), BF16),
            pltpu.VMEM((CHUNKS, rows, 128), F32),
            pltpu.VMEM((CHUNKS, N - 1, rows, 128), F32),
            pltpu.SemaphoreType.DMA((10,)),
            pltpu.SemaphoreType.DMA((10 * CHUNKS,)),
            pltpu.SemaphoreType.DMA((10 * CHUNKS,)),
        ],
        compiler_params=pltpu.CompilerParams(
            collective_id=0, has_side_effects=True, vmem_limit_bytes=67_043_328
        ),
        name="pair",
    )(x, *gains, gate_first.T, up_first.T, down_first, gate_second.T, up_second.T, down_second)
    return out.reshape(tokens, width)


def solution(mesh):
    return jax.shard_map(
        body,
        mesh=mesh,
        in_specs=(
            P(None, "ra"),
            P("ra"),
            P("ra", "cb"),
            P("ra", "cb"),
            P("cb", "ra"),
            P("ra"),
            P("ra", "cb"),
            P("ra", "cb"),
            P("cb", "ra"),
            P("ra"),
        ),
        out_specs=P(None, "ra"),
        check_vma=False,
    )
```

time: 212 us -> 82 us (0.39); the launches traced: 209 us -> 81.9 us
  blocking collectives: 114 us -> 0 us
  Pallas kernels: 0 us -> 80.3 us
  waiting for transfers between devices: 48.1 us -> 0 us
  starting transfers between devices: 23.3 us -> 0 us
  matrix products: 8.6 us -> 0 us
  other arithmetic: 7.07 us -> 0 us
  local copies, waits for them, and re-layouts: 7.42 us -> 1.62 us
    all_to_all x4 -> x0, blocking collectives: 101 us -> none  [the longest x2 72.3 us: sum_at_owner(): lax.all_to_all(in_blocks(value, dim, length), axis, 0, 0, tiled=True)]
    pallas_call x0 -> x1, Pallas kernels: none -> 80.3 us  [body(): pl.pallas_call(kernel, out_shape=jax.ShapeDtypeStruct(x.shape, BF16), in_...]
    all_to_all x4 -> x0, waiting for transfers between devices: 48.1 us -> none  [the longest x2 28.9 us: sum_at_owner(): lax.all_to_all(in_blocks(value, dim, length), axis, 0, 0, tiled=True)]
    all_to_all x4 -> x0, starting transfers between devices: 23.3 us -> none  [the longest x2 16.3 us: sum_at_owner(): lax.all_to_all(in_blocks(value, dim, length), axis, 0, 0, tiled=True)]
    psum x2 -> x0, blocking collectives: 13.7 us -> none  [over_axes(): value = lax.psum(value, axis)]
    dot_general x6 -> x0, matrix products: 8.6 us -> none  [the longest x2 3.66 us: half_step(): gate_part = jnp.dot(normed, w_gate, preferred_element_type=jnp.float32)]
    concatenate x4 -> x0, local copies, waits for them, and re-layouts: 5.83 us -> none  [sent_together(): both = jnp.concatenate(arrays, axis=along)]
    reduce_sum x7 -> x0, other arithmetic: 4.97 us -> none  [the longest x4 3.65 us: sum_at_owner(): return jnp.sum(blocks, axis=0)]
  transfers between devices with their start and end apart: 4 -> 0, of which waited for: 4 -> 0; matrix products, arithmetic and copies ran while one was open for 0% -> 0% of each run, Pallas kernels for 0% -> 0%
where the time goes in v1:
time: 82 us; the launch traced here: 81.9 us
  Pallas kernels  80.3 us (98%)
  local copies, waits for them, and re-layouts  1.62 us (2%)
    pallas_call x1, Pallas kernels, body(): pl.pallas_call(kernel, out_shape=jax.ShapeDtypeStruct(x.shape, BF16), in_...  80.3 us

profile of v1, /device:TPU:1, one launch (start us, length us, event | category | flops | bytes accessed | tf_op | source)
XLA Modules:
  0.0 81.9 jit_solution(16460864353016577231)
XLA Ops:
  0.0 80.3 %pair.1 = bf16[48,8,256]{2,1,0:T(8,128)(2,1)} custom-call(bf16[48,8,256]{2,1,0:T(8,128)(2,1)} %bitcast.11, bf16[256]{0:T(256)(128)(2,1)} %g1.1, bf16[256]{0:T(256)(128)(2,1)} %g2.1, bf16[256]{0:T(256)(128)(2,1)} %g3.1, bf16[704,256]{1,0:T(8,128)(2,1)} %bitcast.7, bf16[704,256]{1,0:T(8,128)(2,1)} %bitcast.8, bf16[704,256]{1,0:T(8,128)(2,1)} %wd1.1, ...), custom_call_target="tpu_custom_call" | custom-call | tf_op jit(solution)/shard_map/pair/pallas_call | solution.py:196
  80.3 1.6 %copy.12 = bf16[384,256]{1,0:T(8,128)(2,1)} copy(bf16[384,256]{1,0:T(8,128)(2,1)} %bitcast.6) | data formatting | bytes 393216
